TPU v7x, 32 devices: a whole 2x2x4 slice. The times are simulated.
32 devices in a mesh: sp: 16 (over z, y, core), tp: 2 (over x).
Axes of the slice: x: 2, y: 2, z: 4, core: 2. Of those that a mesh axis runs over, the one named last changes fastest.
Arguments:
- tokens: bfloat16 [1, 8192, 2048], P(None, ('sp', 'tp')), may hold values from -6 to 6
- input_norm_gain: float32 [2048], replicated, may hold values from 0.1 to 1.9
- query_weight: bfloat16 [2048, 1024], P(None, 'tp'), may hold values from -0.125 to 0.125
- forget_weight: bfloat16 [2048, 1024], P(None, 'tp'), may hold values from -0.125 to 0.125
- input_weight: bfloat16 [2048, 1024], P(None, 'tp'), may hold values from -0.125 to 0.125
- gate_weight: bfloat16 [2048, 1024], P(None, 'tp'), may hold values from -0.125 to 0.125
- slack: float32 [1024], P('tp'), may hold values from 0 to 0.06
- sudden_decay: float32 [1, 8192, 8], P(None, 'sp', 'tp'), may hold values from -0.75 to 0
- head_norm_gain: float32 [128], replicated, may hold values from 0.1 to 1.9
- output_weight: bfloat16 [1024, 2048], P(None, 'tp'), may hold values from -1.25 to 1.25
- output_norm_gain: float32 [2048], P('tp'), may hold values from 0.1 to 1.9
Outputs:
- mixer_output: bfloat16 [1, 8192, 2048], P(None, 'sp', 'tp')
All inputs are finite; a program needn't handle non-finite values.
Results may differ from a plain program's by a relative error of at most 0.0094.
Values may be sent and summed in bfloat16 or wider, within the bound.
A program may use at most 64 MiB of HBM per device.

v0:
```python
import jax
import jax.numpy as jnp
from jax import lax
from jax.sharding import PartitionSpec as P

D = 2048
KEY = 128
BLOCK = 64
epsilon = 1e-06
precise = lax.Precision.HIGHEST


def entering(part, axis, combine, identity):
    place = lax.axis_index(axis)
    gathered = jax.tree.map(lambda a: lax.all_gather(a, axis), part)
    state = jax.tree.map(lambda a, e: jnp.zeros_like(a) + jnp.asarray(e, a.dtype), part, identity)

    def one(turn, state):
        return combine(
            state, jax.tree.map(lambda a: lax.dynamic_index_in_dim(a, turn, 0, False), gathered)
        )

    return lax.fori_loop(0, place, one, state)


def normalize(tensor_in, gain_vec):
    tensor_in = tensor_in.astype(jnp.float32)
    return (
        tensor_in
        * lax.rsqrt(jnp.mean(tensor_in * tensor_in, axis=-1, keepdims=True) + epsilon)
        * gain_vec
    )


def setup_params(query_logits, forget_logits, input_logits, slack, sudden_decay):
    sequence_total, sequence_span, local_heads = sudden_decay.shape

    def heads_first(tensor):
        return (
            tensor.astype(jnp.float32)
            .reshape(sequence_total, sequence_span, local_heads, -1)
            .transpose(0, 2, 1, 3)
        )

    query_rows = heads_first(query_logits) * KEY ** (-0.5)
    incoming_weights = slack.reshape(local_heads, -1)[None, :, None, :] * jax.nn.sigmoid(
        -heads_first(forget_logits)
    )
    forget_logarithm = jnp.log1p(-incoming_weights) + sudden_decay.transpose(0, 2, 1)[:, :, :, None]
    return (query_rows, incoming_weights, heads_first(input_logits), forget_logarithm)


def block_pass(query_rows, incoming_weights, value_rows, forget_logarithm, initial):
    sequence_total, local_heads, sequence_span, key_width = query_rows.shape
    blocks_here = sequence_span // BLOCK

    def by_block(tensor):
        return tensor.reshape(
            sequence_total, local_heads, blocks_here, BLOCK, tensor.shape[3]
        ).transpose(2, 0, 1, 3, 4)

    causal = jnp.tril(jnp.ones((BLOCK, BLOCK), dtype=bool))

    def advance(carried, portions):
        query_blk, weight_blk, value_blk, forget_blk = portions
        running = jnp.cumsum(forget_blk, axis=2)
        lifted_q = query_blk * jnp.exp(running)
        lifted_k = weight_blk * jnp.exp(-running)
        scores = jnp.einsum("shtk,shuk->shtu", lifted_q, lifted_k, precision=precise)
        scores = jnp.where(causal, scores, 0.0)
        produced = jnp.einsum("shtu,shuv->shtv", scores, value_blk, precision=precise) + jnp.einsum(
            "shtk,shkv->shtv", lifted_q, carried, precision=precise
        )
        ending = running[:, :, -1:, :]
        carried = jnp.exp(ending[:, :, 0, :])[..., None] * carried + jnp.einsum(
            "shuk,shuv->shkv", weight_blk * jnp.exp(ending - running), value_blk, precision=precise
        )
        return (carried, produced)

    final_state, produced = lax.scan(
        advance,
        initial,
        (
            by_block(query_rows),
            by_block(incoming_weights),
            by_block(value_rows),
            by_block(forget_logarithm),
        ),
    )
    return (
        final_state,
        produced.transpose(1, 2, 0, 3, 4).reshape(
            sequence_total, local_heads, sequence_span, value_rows.shape[3]
        ),
    )


def gate_heads(produced, gate_raw, head_norm_gain):
    sequence_total, local_heads, sequence_span, val_width = produced.shape
    mean_sq = jnp.mean(produced * produced, axis=3, keepdims=True)
    scaled = produced * lax.rsqrt(mean_sq + epsilon) * head_norm_gain
    scaled = scaled.transpose(0, 2, 1, 3).reshape(
        sequence_total, sequence_span, local_heads * val_width
    )
    return (scaled * jax.nn.silu(gate_raw.astype(jnp.float32))).astype(jnp.bfloat16)


def join_states(earlier, later):
    earlier_decay, earlier_state = earlier
    later_decay, later_state = later
    return (
        earlier_decay + later_decay,
        jnp.exp(later_decay)[..., None] * earlier_state + later_state,
    )


def recurrence(query_rows, incoming_weights, value_rows, forget_logarithm):
    sequence_total, local_heads, sequence_span, key_width = query_rows.shape
    val_width = value_rows.shape[3]
    through = jnp.cumsum(forget_logarithm, axis=2)
    totals = through[:, :, -1, :]
    head_spans = (0, local_heads)
    head_from, head_upto = head_spans
    zero_state = jnp.zeros(
        (sequence_total, head_upto - head_from, key_width, val_width), jnp.float32
    )
    final_state, produced = block_pass(
        query_rows, incoming_weights, value_rows, forget_logarithm, zero_state
    )
    identity = (jnp.zeros_like(totals), jnp.zeros_like(final_state))
    incoming = entering((totals, final_state), "sp", join_states, identity)
    incoming = incoming[1]
    readout = jnp.einsum(
        "shtk,shkv->shtv", query_rows * jnp.exp(through), incoming, precision=precise
    )
    outputs = produced + readout
    return outputs


def shards(
    tokens,
    input_norm_gain,
    query_weight,
    forget_weight,
    input_weight,
    gate_weight,
    slack,
    sudden_decay,
    head_norm_gain,
    output_weight,
    output_norm_gain,
):
    normed = normalize(tokens, input_norm_gain).astype(jnp.bfloat16)
    matrices = (query_weight, forget_weight, input_weight, gate_weight)
    portion = lax.all_gather(normed, "tp", axis=1, tiled=True)
    joined = lax.optimization_barrier(
        jnp.concatenate(
            [
                jnp.einsum(
                    "std,dc->stc", portion, matrix, preferred_element_type=jnp.float32
                ).astype(jnp.bfloat16)
                for matrix in matrices
            ],
            axis=2,
        )
    )
    query_cols = query_weight.shape[1]
    input_cols = input_weight.shape[1]
    query_logits = joined[:, :, :query_cols]
    forget_logits = joined[:, :, query_cols : 2 * query_cols]
    input_logits = joined[:, :, 2 * query_cols : 2 * query_cols + input_cols]
    gate_raw = joined[:, :, 2 * query_cols + input_cols :]
    query_rows, incoming_weights, value_rows, forget_logarithm = setup_params(
        query_logits, forget_logits, input_logits, slack, sudden_decay
    )
    produced = recurrence(query_rows, incoming_weights, value_rows, forget_logarithm)
    gated_out = gate_heads(produced, gate_raw, head_norm_gain)
    projected = jnp.einsum(
        "stc,cd->std",
        lax.all_gather(gated_out, "tp", axis=2, tiled=True),
        output_weight,
        preferred_element_type=jnp.float32,
    )
    squares = lax.psum(jnp.sum(projected * projected, axis=2, keepdims=True), "tp")
    return (projected * lax.rsqrt(squares / D + epsilon) * output_norm_gain).astype(jnp.bfloat16)


def solution(mesh):
    placed = (
        P(None, ("sp", "tp"), None),
        P(),
        P(None, "tp"),
        P(None, "tp"),
        P(None, "tp"),
        P(None, "tp"),
        P("tp"),
        P(None, "sp", "tp"),
        P(),
        P(None, "tp"),
        P("tp"),
    )
    return jax.shard_map(
        shards, mesh=mesh, in_specs=placed, out_specs=P(None, "sp", "tp"), check_vma=False
    )
```

profile of v0, /device:TPU:0, one launch (start us, length us, event | category | flops | bytes accessed | tf_op | source)
XLA Modules:
  0.0 237.6 jit_solution(12733148455241337241)
XLA Ops:
  6.5 1.7 fusion.26
  8.2 2.5 %fusion.28 = bf16[1,256,2048]{2,1,0:T(8,128)(2,1)} fusion(bf16[1,256,2048]{2,1,0:T(8,128)(2,1)} %param.15, f32[2048]{0:T(1024)} %param.16, f32[256]{0:T(256)S(1)} %add_rsqrt_fusion.2), kind=kLoop, calls=%fused_computation.40 | loop fusion | flops 2097152 | bytes 2106368 | tf_op jit(solution)/shard_map/convert_element_type | solution.py:153
  10.8 35.9 %all-gather.6.cloned.1.call-done = bf16[1,512,2048]{2,1,0:T(8,128)(2,1)} async-done(((bf16[1,256,2048]{2,1,0:T(8,128)(2,1)}), bf16[1,512,2048]{2,1,0:T(8,128)(2,1)}) %all-gather.6.cloned.1.call-update) | async-done | bytes 2097168 | tf_op jit(solution)/shard_map/all_gather | solution.py:155
  46.7 3.7 %fusion.49 = bf16[1,512,512]{1,2,0:T(8,128)(2,1)S(1)} fusion(bf16[2048,512]{1,0:T(8,128)(2,1)} %param.20, bf16[1,512,2048]{2,1,0:T(8,128)(2,1)} %all-gather.6.cloned.1.call-done), kind=kOutput, calls=%fused_computation.59 | convolution fusion | flops 1074003968 | bytes 4718592 | tf_op jit(solution)/shard_map/std,dc->stc/dot_general | solution.py:159
  50.4 1.3 fusion.52
  52.0 1.3 fusion.55
  53.6 1.3 fusion.58
  55.0 1.4 convert_multiply_fusion.3
  56.7 1.3 copy.32
  58.0 3.1 %bitcast_add_fusion.2 = (f32[1,4,128,512]{2,3,1,0:T(8,128)}, f32[1,512,4,128]{3,1,2,0:T(8,128)}) fusion(f32[4,512]{1,0:T(4,128)S(1)} %bitcast.243, f32[1,512,4,128]{3,1,2,0:T(8,128)} %copy.32, f32[4,128]{1,0:T(4,128)S(1)} %bitcast.248), kind=kLoop, calls=%fused_computation.72 | loop fusion | flops 786432 | bytes 3155968 | tf_op jit(solution)/shard_map/add | solution.py:49
  61.1 2.6 %fusion.70 = f32[1,4,512,128]{3,2,1,0:T(8,128)} fusion(f32[1,512,4,128]{3,1,2,0:T(8,128)} %get-tuple-element.175, f32[4,512]{1,0:T(4,128)S(1)} %bitcast.244), kind=kLoop, calls=%fused_computation.76 | loop fusion | flops 524288 | bytes 2105344 | tf_op jit(solution)/shard_map/add | solution.py:49
  63.7 1.2 copy.33
  64.9 2.6 %copy.34 = f32[1,512,4,128]{3,1,2,0:T(8,128)} copy(f32[1,512,4,128]{1,3,2,0:T(8,128)} %bitcast.233) | data formatting | bytes 2097152 | tf_op jit(solution)/shard_map/mul | solution.py:45
  67.4 57.5 %while.26 = (s32[]{:T(128)}, f32[1,4,128,128]{3,2,1,0:T(8,128)S(1)}, f32[8,1,4,64,128]{4,3,0,2,1:T(8,128)}, f32[8,1,4,64,128]{4,3,0,2,1:T(8,128)}, f32[8,1,4,64,...) while((s32[]{:T(128)}, ...), condition=%wide.region_3.4_spmd.clone, body=%wide.region_1.3_spmd.clone.sunk | while | flops 153571328 | bytes 3174530 | solution.py:80
  68.5 1.3 convolution_select_fusion.2
  69.9 1.2 fusion.95
  71.0 1.9 fusion.96
  73.0 1.6 fusion.94
  74.6 0.9 dynamic-slice_bitcast_fusion.2
  75.7 1.3 convolution_select_fusion.2
  77.1 1.2 fusion.95
  78.2 1.9 fusion.96
  80.2 1.6 fusion.94
  81.8 0.9 dynamic-slice_bitcast_fusion.2
  82.9 1.3 convolution_select_fusion.2
  84.2 1.2 fusion.95
  85.4 1.9 fusion.96
  87.4 1.6 fusion.94
  89.0 0.9 dynamic-slice_bitcast_fusion.2
  90.1 1.3 convolution_select_fusion.2
  91.4 1.2 fusion.95
  92.6 1.9 fusion.96
  94.6 1.6 fusion.94
  96.2 0.9 dynamic-slice_bitcast_fusion.2
  97.3 1.3 convolution_select_fusion.2
  98.6 1.2 fusion.95
  99.8 1.9 fusion.96
  101.8 1.6 fusion.94
  103.4 0.9 dynamic-slice_bitcast_fusion.2
  104.5 1.3 convolution_select_fusion.2
  105.8 1.2 fusion.95
  107.0 1.9 fusion.96
  109.0 1.6 fusion.94
  110.6 0.9 dynamic-slice_bitcast_fusion.2
  111.7 1.3 convolution_select_fusion.2
  113.0 1.2 fusion.95
  114.2 1.9 fusion.96
  116.2 1.6 fusion.94
  118.9 1.3 convolution_select_fusion.2
  120.2 1.2 fusion.95
  121.4 1.9 fusion.96
  123.3 1.6 fusion.94
  125.8 2.5 %copy.46 = f32[4,512,128]{1,2,0:T(8,128)} copy(f32[4,512,128]{2,1,0:T(8,128)} %bitcast.238) | data formatting | bytes 2097152 | tf_op jit(solution)/shard_map/reshape | solution.py:92
  129.3 1.0 copy-done.5
  130.3 21.6 %all-gather = f32[16,4,1,128]{3,1,2,0:T(4,128)S(1)} all-gather(f32[1,4,1,128]{3,1,2,0:T(4,128)S(1)} %bitcast.246), channel_id=2, replica_groups=mesh['sp'=16,'tp'=2] {'sp'}, dimensions={0}, use_global_device_ids=true | all-gather | bytes 34816 | tf_op jit(solution)/shard_map/all_gather | solution.py:15
  151.8 24.5 %all-gather.10.cloned.1.call-done = f32[16,4,128,128]{3,2,1,0:T(8,128)} async-done(((f32[1,4,128,128]{3,2,1,0:T(8,128)}), f32[16,4,128,128]{3,2,1,0:T(8,128)}) %all-gather.10.cloned.1.call-update) | async-done | bytes 4194320 | tf_op jit(solution)/shard_map/all_gather | solution.py:15
  176.6 1.0 copy-done.2
  177.6 2.9 %multiply_reduce_fusion.1 = (f32[4,512]{1,0:T(4,128)S(1)}, f32[4,512,128]{1,2,0:T(8,128)S(1)}) fusion(f32[4,512,128]{1,2,0:T(8,128)} %copy.46, f32[1,4,128,128]{3,2,1,0:T(8,128)S(1)} %get-tuple-element.94, f32[1,512,4,128]{3,1,2,0:T(8,128)S(1)} %bitcast.229, f32[1,4,128,512]{2,3,1,0:T(8,128)} %copy-done.5), kind=kOutput, calls=%fused_computation.80 | convolution fusion | flops 403699712 | bytes 4464640 | tf_op jit(solution)/shard_map/shtk,shkv->shtv/dot_general | solution.py:133
  180.7 1.4 copy-done.4
  182.0 1.1 fusion.74
  183.2 36.3 %all-gather.8.cloned.1.call-done = bf16[1,512,1024]{1,2,0:T(8,128)(2,1)} async-done(((bf16[1,512,512]{1,2,0:T(8,128)(2,1)}), bf16[1,512,1024]{1,2,0:T(8,128)(2,1)}) %all-gather.8.cloned.1.call-update) | async-done | bytes 1048592 | tf_op jit(solution)/shard_map/all_gather | solution.py:180
  219.5 3.8 %multiply_reduce_fusion = (f32[512]{0:T(512)S(1)}, f32[512,1024]{1,0:T(8,128)}) fusion(bf16[1024,1024]{1,0:T(8,128)(2,1)S(1)} %copy-done, bf16[1,512,1024]{1,2,0:T(8,128)(2,1)} %all-gather.8.cloned.1.call-done), kind=kOutput, calls=%fused_computation.51 | convolution fusion | flops 1074789888 | bytes 5244928 | tf_op jit(solution)/shard_map/stc,cd->std/dot_general | solution.py:178
  223.3 4.9 %psum.7 = f32[1,512,1]{1,2,0:T(1,128)S(1)} all-reduce(f32[1,512,1]{1,2,0:T(1,128)S(1)} %bitcast.245), channel_id=1, replica_groups=mesh['sp'=16,'tp'=2] {'tp'}, use_global_device_ids=true, to_apply=%region_10.11 | all-reduce | flops 512 | bytes 4096 | tf_op jit(solution)/shard_map/psum | solution.py:184
  228.2 2.8 %fusion.65 = bf16[1,512,1024]{2,1,0:T(8,128)(2,1)} fusion(f32[512,1024]{1,0:T(8,128)} %get-tuple-element.181, f32[1024]{0:T(1024)S(1)} %copy-done.8, f32[512]{0:T(512)S(1)} %bitcast.247), kind=kLoop, calls=%fused_computation.67 | loop fusion | flops 1572864 | bytes 3151872 | tf_op jit(solution)/shard_map/convert_element_type | solution.py:185
  (85 shorter events, 6.3 us)
Async XLA Ops:
  6.5 212.9 %copy-start = (bf16[1024,1024]{1,0:T(8,128)(2,1)S(1)}, bf16[1024,1024]{1,0:T(8,128)(2,1)}, u32[]{:S(2)}) copy-start(bf16[1024,1024]{1,0:T(8,128)(2,1)} %param.24) | copy-start | bytes 6291460
  6.5 40.2 %all-gather.6.cloned.1.call-start = ((), (), s32[]{:S(2)}) async-start(), calls=%async_computation | async-start | bytes 3145728 | tf_op jit(solution)/shard_map/all_gather | solution.py:155
  10.7 165.6 %all-gather.10.cloned.1.call-start = ((), (), s32[]{:S(2)}) async-start(), calls=%async_computation.2 | async-start | bytes 4456448 | tf_op jit(solution)/shard_map/all_gather | solution.py:15
  46.7 3.7 %copy-start.11 = (bf16[2048,512]{1,0:T(8,128)(2,1)S(1)}, bf16[2048,512]{1,0:T(8,128)(2,1)}, u32[]{:S(2)}) copy-start(bf16[2048,512]{1,0:T(8,128)(2,1)} %param.19) | copy-start | bytes 6291460
  46.7 3.7 %copy-start.14 = (bf16[1,512,2048]{2,1,0:T(8,128)(2,1)S(1)}, bf16[1,512,2048]{2,1,0:T(8,128)(2,1)}, u32[]{:S(2)}) copy-start(bf16[1,512,2048]{2,1,0:T(8,128)(2,1)} %all-gather.6.cloned.1.call-done) | copy-start | bytes 6291460
  50.4 1.6 copy-start.12
  52.0 1.6 copy-start.13
  55.0 1.7 copy-start.3
  56.5 1.6 copy-start.7
  56.5 1.6 copy-start.9
  58.0 5.6 %slice-start = ((bf16[1,512,2048]{1,2,0:T(8,128)(2,1)}), bf16[1,512,512]{1,2,0:T(8,128)(2,1)S(1)}, s32[]{:S(2)}) async-start(bf16[1,512,2048]{1,2,0:T(8,128)(2,1)} %copy-done.3), calls=%async_computation.3 | async-start | bytes 1048576 | tf_op jit(solution)/shard_map/slice | solution.py:171
  125.0 0.7 copy-start.1
  125.0 3.3 %copy-start.6 = (f32[1,4,128,512]{2,3,1,0:T(8,128)S(1)}, f32[1,4,128,512]{2,3,1,0:T(8,128)}, u32[]{:S(2)}) copy-start(f32[1,4,128,512]{2,3,1,0:T(8,128)} %get-tuple-element.174) | copy-start | bytes 3145732
  125.7 93.7 %all-gather.8.cloned.1.call-start = ((), (), s32[]{:S(2)}) async-start(), calls=%async_computation.1 | async-start | bytes 1572864 | tf_op jit(solution)/shard_map/all_gather | solution.py:180
  129.2 1.0 copy-start.5
  176.3 1.2 copy-start.2
  177.6 2.9 %copy-start.10 = (f32[128]{0:T(128)S(1)}, f32[128]{0:T(128)}, u32[]{:S(2)}) copy-start(f32[128]{0:T(128)} %param.23) | copy-start | bytes 1540
  180.4 1.6 copy-start.4
  183.2 45.1 %copy-start.8 = (f32[1024]{0:T(1024)S(1)}, f32[1024]{0:T(1024)}, u32[]{:S(2)}) copy-start(f32[1024]{0:T(1024)} %param.25) | copy-start | bytes 12292
Sparse Core Ops, SparseCore 0:
  10.9 35.8 all-gather.5
  125.8 50.4 all-gather.9
  183.3 36.1 all-gather.7
where the time goes:
time: 239 us; the launch traced here: 238 us
  waiting for transfers between devices  96.8 us (41%)
  matrix products  62.7 us (26%)
  blocking collectives  26.5 us (11%)
  local copies, waits for them, and re-layouts  20.1 us (8%)
  other arithmetic  17.5 us (7%)
  between operations  13.3 us (6%)
    all_gather x1, waiting for transfers between devices, shards(): lax.all_gather(gated_out, 'tp', axis=2, tiled=True)  36.3 us
    all_gather x1, waiting for transfers between devices, shards(): portion = lax.all_gather(normed, 'tp', axis=1, tiled=True)  35.9 us
    all_gather x1, waiting for transfers between devices, entering(): gathered = jax.tree.map(lambda a: lax.all_gather(a, axis), part)  24.5 us
    all_gather x1, blocking collectives, entering(): gathered = jax.tree.map(lambda a: lax.all_gather(a, axis), part)  21.6 us
    dot_general x8, matrix products, advance(): jnp.einsum('shtk,shkv->shtv', lifted_q, carried, precision=precise)  15.5 us
    dot_general x8, matrix products, advance(): jnp.einsum('shuk,shuv->shkv', weight_blk * jnp.exp(ending - running), val...  13 us
    dot_general x8, matrix products, advance(): jnp.einsum('shtk,shuk->shtu', lifted_q, lifted_k, precision=precise)  10.6 us
    dot_general x8, matrix products, advance(): jnp.einsum('shtu,shuv->shtv', scores, value_blk, precision=precise)  9.35 us
  transfers between devices with their start and end apart: 3, of which 3 were waited for; matrix products, arithmetic and copies ran while one was open for 1% of the time, Pallas kernels for 0%

commit v1 on v0

--- a/solution.py
+++ b/solution.py
@@ -8,6 +8,18 @@
 BLOCK = 64
 epsilon = 1e-06
 precise = lax.Precision.HIGHEST
+
+
+def ring_product(value, axis, dim, product):
+    size, index = (lax.axis_size(axis), lax.axis_index(axis))
+    left = [(i, (i - 1) % size) for i in range(size)]
+    span = value.shape[dim]
+    held = value
+    running = product(held, index * span)
+    for step in range(1, size):
+        held = lax.ppermute(held, axis, left)
+        running = running + product(held, (index + step) % size * span)
+    return running
 
 
 def entering(part, axis, combine, identity):
@@ -175,11 +187,16 @@
     )
     produced = recurrence(query_rows, incoming_weights, value_rows, forget_logarithm)
     gated_out = gate_heads(produced, gate_raw, head_norm_gain)
-    projected = jnp.einsum(
-        "stc,cd->std",
-        lax.all_gather(gated_out, "tp", axis=2, tiled=True),
-        output_weight,
-        preferred_element_type=jnp.float32,
+    projected = ring_product(
+        gated_out,
+        "tp",
+        2,
+        lambda shard, start: jnp.einsum(
+            "stc,cd->std",
+            shard,
+            lax.dynamic_slice_in_dim(output_weight, start, shard.shape[2], axis=0),
+            preferred_element_type=jnp.float32,
+        ),
     )
     squares = lax.psum(jnp.sum(projected * projected, axis=2, keepdims=True), "tp")
     return (projected * lax.rsqrt(squares / D + epsilon) * output_norm_gain).astype(jnp.bfloat16)

time: 239 us -> 226 us (0.946)
  the two profiles are of different devices: /device:TPU:0 before, /device:TPU:28 now
where the time goes in v1:
time: 226 us; the launch traced here: 225 us
  waiting for transfers between devices  73.4 us (32%)
  matrix products  61.7 us (27%)
  other arithmetic  32.3 us (14%)
  blocking collectives  21.7 us (10%)
  local copies, waits for them, and re-layouts  19.3 us (9%)
  between operations  13.7 us (6%)
    all_gather x1, waiting for transfers between devices, shards(): portion = lax.all_gather(normed, 'tp', axis=1, tiled=True)  34.1 us
    all_gather x1, waiting for transfers between devices, entering(): gathered = jax.tree.map(lambda a: lax.all_gather(a, axis), part)  27.1 us
    all_gather x1, blocking collectives, entering(): gathered = jax.tree.map(lambda a: lax.all_gather(a, axis), part)  16.7 us
    add x14, other arithmetic, join_states(): jnp.exp(later_decay)[..., None] * earlier_state + later_state  15.7 us
    dot_general x8, matrix products, advance(): jnp.einsum('shtk,shkv->shtv', lifted_q, carried, precision=precise)  15.5 us
    dot_general x8, matrix products, advance(): jnp.einsum('shuk,shuv->shkv', weight_blk * jnp.exp(ending - running), val...  13 us
    ppermute x1, waiting for transfers between devices, ring_product(): held = lax.ppermute(held, axis, left)  12.2 us
    dot_general x8, matrix products, advance(): jnp.einsum('shtk,shuk->shtu', lifted_q, lifted_k, precision=precise)  10.6 us
  transfers between devices with their start and end apart: 3, of which 3 were waited for; matrix products, arithmetic and copies ran while one was open for 2% of the time, Pallas kernels for 0%

profile of v1, /device:TPU:28, one launch (start us, length us, event | category | flops | bytes accessed | tf_op | source)
XLA Modules:
  0.0 224.7 jit_solution(2842859089587822508)
XLA Ops:
  6.5 1.7 fusion.26
  8.2 2.5 %fusion.28 = bf16[1,256,2048]{2,1,0:T(8,128)(2,1)} fusion(bf16[1,256,2048]{2,1,0:T(8,128)(2,1)} %param.15, f32[2048]{0:T(1024)} %param.16, f32[256]{0:T(256)S(1)} %add_rsqrt_fusion.2), kind=kLoop, calls=%fused_computation.40 | loop fusion | flops 2097152 | bytes 2106368 | tf_op jit(solution)/shard_map/convert_element_type | solution.py:165
  10.8 34.1 %all-gather.5.cloned.1.call-done = bf16[1,512,2048]{2,1,0:T(8,128)(2,1)} async-done(((bf16[1,256,2048]{2,1,0:T(8,128)(2,1)}), bf16[1,512,2048]{2,1,0:T(8,128)(2,1)}) %all-gather.5.cloned.1.call-update) | async-done | bytes 2097168 | tf_op jit(solution)/shard_map/all_gather | solution.py:167
  44.9 3.7 %fusion.49 = bf16[1,512,512]{1,2,0:T(8,128)(2,1)S(1)} fusion(bf16[2048,512]{1,0:T(8,128)(2,1)} %param.20, bf16[1,512,2048]{2,1,0:T(8,128)(2,1)} %all-gather.5.cloned.1.call-done), kind=kOutput, calls=%fused_computation.60 | convolution fusion | flops 1074003968 | bytes 4718592 | tf_op jit(solution)/shard_map/std,dc->stc/dot_general | solution.py:171
  48.6 1.3 fusion.52
  50.2 1.3 fusion.55
  51.8 1.3 fusion.58
  53.3 1.4 convert_multiply_fusion.3
  54.9 1.3 copy.32
  56.2 3.1 %bitcast_add_fusion.2 = (f32[1,4,128,512]{2,3,1,0:T(8,128)}, f32[1,512,4,128]{3,1,2,0:T(8,128)}) fusion(f32[4,512]{1,0:T(4,128)S(1)} %bitcast.245, f32[1,512,4,128]{3,1,2,0:T(8,128)} %copy.32, f32[4,128]{1,0:T(4,128)S(1)} %bitcast.250), kind=kLoop, calls=%fused_computation.71 | loop fusion | flops 786432 | bytes 3155968 | tf_op jit(solution)/shard_map/add | solution.py:61
  59.3 2.6 %fusion.68 = f32[1,4,512,128]{3,2,1,0:T(8,128)} fusion(f32[1,512,4,128]{3,1,2,0:T(8,128)} %get-tuple-element.175, f32[4,512]{1,0:T(4,128)S(1)} %bitcast.246), kind=kLoop, calls=%fused_computation.75 | loop fusion | flops 524288 | bytes 2105344 | tf_op jit(solution)/shard_map/add | solution.py:61
  61.9 1.2 copy.33
  63.1 2.5 %copy.34 = f32[1,512,4,128]{3,1,2,0:T(8,128)} copy(f32[1,512,4,128]{1,3,2,0:T(8,128)} %bitcast.235) | data formatting | bytes 2097152 | tf_op jit(solution)/shard_map/mul | solution.py:57
  65.6 57.5 %while.26 = (s32[]{:T(128)}, f32[1,4,128,128]{3,2,1,0:T(8,128)S(1)}, f32[8,1,4,64,128]{4,3,0,2,1:T(8,128)}, f32[8,1,4,64,128]{4,3,0,2,1:T(8,128)}, f32[8,1,4,64,...) while((s32[]{:T(128)}, ...), condition=%wide.region_3.4_spmd.clone, body=%wide.region_1.3_spmd.clone.sunk | while | flops 153571328 | bytes 3174530 | solution.py:92
  66.7 1.3 convolution_select_fusion.2
  68.0 1.2 fusion.99
  69.2 1.9 fusion.100
  71.2 1.6 fusion.98
  73.9 1.3 convolution_select_fusion.2
  75.2 1.2 fusion.99
  76.4 1.9 fusion.100
  78.4 1.6 fusion.98
  81.1 1.3 convolution_select_fusion.2
  82.4 1.2 fusion.99
  83.6 1.9 fusion.100
  85.6 1.6 fusion.98
  88.3 1.3 convolution_select_fusion.2
  89.6 1.2 fusion.99
  90.8 1.9 fusion.100
  92.7 1.6 fusion.98
  95.5 1.3 convolution_select_fusion.2
  96.8 1.2 fusion.99
  98.0 1.9 fusion.100
  99.9 1.6 fusion.98
  102.7 1.3 convolution_select_fusion.2
  104.0 1.2 fusion.99
  105.2 1.9 fusion.100
  107.1 1.6 fusion.98
  109.9 1.3 convolution_select_fusion.2
  111.2 1.2 fusion.99
  112.4 1.9 fusion.100
  114.3 1.6 fusion.98
  117.1 1.3 convolution_select_fusion.2
  118.4 1.2 fusion.99
  119.6 1.9 fusion.100
  121.5 1.6 fusion.98
  123.9 2.5 %copy.46 = f32[4,512,128]{1,2,0:T(8,128)} copy(f32[4,512,128]{2,1,0:T(8,128)} %bitcast.240) | data formatting | bytes 2097152 | tf_op jit(solution)/shard_map/reshape | solution.py:104
  128.4 16.7 %all-gather = f32[16,4,1,128]{3,1,2,0:T(4,128)S(1)} all-gather(f32[1,4,1,128]{3,1,2,0:T(4,128)S(1)} %bitcast.248), channel_id=2, replica_groups=mesh['sp'=16,'tp'=2] {'sp'}, dimensions={0}, use_global_device_ids=true | all-gather | bytes 34816 | tf_op jit(solution)/shard_map/all_gather | solution.py:27
  145.2 27.1 %all-gather.7.cloned.1.call-done = f32[16,4,128,128]{3,2,1,0:T(8,128)} async-done(((f32[1,4,128,128]{3,2,1,0:T(8,128)}), f32[16,4,128,128]{3,2,1,0:T(8,128)}) %all-gather.7.cloned.1.call-update) | async-done | bytes 4194320 | tf_op jit(solution)/shard_map/all_gather | solution.py:27
  172.3 16.5 %while.25 = (s32[]{:T(128)}, f32[1,4,128,128]{3,2,1,0:T(8,128)S(1)}, s32[]{:T(128)}, f32[16,1,4,128]{3,2,1,0:T(4,128)S(1)}, f32[16,1,4,128,128]{4,3,2,1,0:T(8,128)}, /*index=5*/s32[]{:T(128)}, s32[]{:T(128)}, s32[]{:T(128)}) while((s32[]{:T(128)}, f32[1,4,128,128]{3,2,1,0:T(8,128)S(1)}, s32[]{:T(128)}, f32[16,1,4,128]{3,2,1,0:T(4,128)S(1)}, ...), condition=%wide.region_7.8_spmd, body=%wide.region_6.7_spmd.sunk | while | flops 131077 | bytes 792711 | solution.py:35
  172.4 1.2 bitcast_add_fusion.4
  173.6 1.1 bitcast_add_fusion.4
  174.8 1.1 bitcast_add_fusion.4
  175.9 1.1 bitcast_add_fusion.4
  185.2 1.1 bitcast_add_fusion.4
  186.3 1.1 bitcast_add_fusion.4
  187.5 1.1 bitcast_add_fusion.4
  188.8 2.9 %multiply_reduce_fusion.1 = (f32[4,512]{1,0:T(4,128)S(1)}, f32[4,512,128]{1,2,0:T(8,128)S(1)}) fusion(f32[4,512,128]{1,2,0:T(8,128)} %copy.46, f32[1,4,128,128]{3,2,1,0:T(8,128)S(1)} %get-tuple-element.94, f32[1,512,4,128]{3,1,2,0:T(8,128)S(1)} %bitcast.231, f32[1,4,128,512]{2,3,1,0:T(8,128)} %copy-done.5), kind=kOutput, calls=%fused_computation.82 | convolution fusion | flops 403699712 | bytes 4464640 | tf_op jit(solution)/shard_map/shtk,shkv->shtv/dot_general | solution.py:145
  191.9 1.4 copy-done.4
  193.6 1.5 collective-permute-start
  195.9 12.2 %collective-permute-done = bf16[1,512,512]{1,2,0:T(8,128)(2,1)S(1)} collective-permute-done((bf16[1,512,512]{1,2,0:T(8,128)(2,1)S(1)}, bf16[1,512,512]{1,2,0:T(8,128)(2,1)S(1)}, u32[]{:S(2)}, u32[]{:S(2)}) %collective-permute-start) | collective-permute-done | bytes 524320 | tf_op jit(solution)/shard_map/ppermute | solution.py:20
  208.0 2.1 multiply_reduce_fusion
  210.1 4.9 %psum.7 = f32[1,512,1]{1,2,0:T(1,128)S(1)} all-reduce(f32[1,512,1]{1,2,0:T(1,128)S(1)} %bitcast.247), channel_id=1, replica_groups=mesh['sp'=16,'tp'=2] {'tp'}, use_global_device_ids=true, to_apply=%region_10.11 | all-reduce | flops 512 | bytes 4096 | tf_op jit(solution)/shard_map/psum | solution.py:201
  215.0 2.8 %fusion.65 = bf16[1,512,1024]{2,1,0:T(8,128)(2,1)} fusion(f32[512,1024]{1,0:T(8,128)} %get-tuple-element.181, f32[1024]{0:T(1024)S(1)} %copy-done.8, f32[512]{0:T(512)S(1)} %bitcast.249), kind=kLoop, calls=%fused_computation.68 | loop fusion | flops 1572864 | bytes 3151872 | tf_op jit(solution)/shard_map/convert_element_type | solution.py:202
  (113 shorter events, 21.6 us)
Async XLA Ops:
  6.5 188.6 %copy-start = (bf16[1024,1024]{1,0:T(8,128)(2,1)S(1)}, bf16[1024,1024]{1,0:T(8,128)(2,1)}, u32[]{:S(2)}) copy-start(bf16[1024,1024]{1,0:T(8,128)(2,1)} %param.24) | copy-start | bytes 6291460
  6.5 38.4 %all-gather.5.cloned.1.call-start = ((), (), s32[]{:S(2)}) async-start(), calls=%async_computation | async-start | bytes 3145728 | tf_op jit(solution)/shard_map/all_gather | solution.py:167
  10.7 161.6 %all-gather.7.cloned.1.call-start = ((), (), s32[]{:S(2)}) async-start(), calls=%async_computation.1 | async-start | bytes 4456448 | tf_op jit(solution)/shard_map/all_gather | solution.py:27
  44.9 3.7 %copy-start.11 = (bf16[2048,512]{1,0:T(8,128)(2,1)S(1)}, bf16[2048,512]{1,0:T(8,128)(2,1)}, u32[]{:S(2)}) copy-start(bf16[2048,512]{1,0:T(8,128)(2,1)} %param.19) | copy-start | bytes 6291460
  44.9 3.7 %copy-start.14 = (bf16[1,512,2048]{2,1,0:T(8,128)(2,1)S(1)}, bf16[1,512,2048]{2,1,0:T(8,128)(2,1)}, u32[]{:S(2)}) copy-start(bf16[1,512,2048]{2,1,0:T(8,128)(2,1)} %all-gather.5.cloned.1.call-done) | copy-start | bytes 6291460
  48.6 1.6 copy-start.12
  50.2 1.6 copy-start.13
  53.2 1.7 copy-start.3
  54.7 1.5 copy-start.7
  54.7 1.5 copy-start.9
  56.2 5.6 %slice-start = ((bf16[1,512,2048]{1,2,0:T(8,128)(2,1)}), bf16[1,512,512]{1,2,0:T(8,128)(2,1)S(1)}, s32[]{:S(2)}) async-start(bf16[1,512,2048]{1,2,0:T(8,128)(2,1)} %copy-done.3), calls=%async_computation.2 | async-start | bytes 1048576 | tf_op jit(solution)/shard_map/slice | solution.py:183
  123.2 0.7 copy-start.1
  123.2 3.3 %copy-start.6 = (f32[1,4,128,512]{2,3,1,0:T(8,128)S(1)}, f32[1,4,128,512]{2,3,1,0:T(8,128)}, u32[]{:S(2)}) copy-start(f32[1,4,128,512]{2,3,1,0:T(8,128)} %get-tuple-element.174) | copy-start | bytes 3145732
  127.4 1.0 copy-start.5
  172.3 16.5 %copy-start.2 = (f32[8,1,4,64,128]{4,3,0,2,1:T(8,128)S(1)}, f32[8,1,4,64,128]{4,3,0,2,1:T(8,128)}, u32[]{:S(2)}) copy-start(f32[8,1,4,64,128]{4,3,0,2,1:T(8,128)} %get-tuple-element.315) | copy-start | bytes 3145732
  188.8 2.9 %copy-start.10 = (f32[128]{0:T(128)S(1)}, f32[128]{0:T(128)}, u32[]{:S(2)}) copy-start(f32[128]{0:T(128)} %param.23) | copy-start | bytes 1540
  191.7 1.6 copy-start.4
  193.6 14.4 %collective-permute-start = (bf16[1,512,512]{1,2,0:T(8,128)(2,1)S(1)}, bf16[1,512,512]{1,2,0:T(8,128)(2,1)S(1)}, u32[]{:S(2)}, u32[]{:S(2)}) collective-permute-start(bf16[1,512,512]{1,2,0:T(8,128)(2,1)S(1)} %fusion.75), channel_id=1, source_target_pairs={{0,1},{1,0},{2,3},{3,2},{4,5},{5,4},{6,7},{7,6},{8,9},{9,8},{10,11... | collective-permute-start | bytes 1572872 | tf_op jit(solution)/shard_map/ppermute | solution.py:20
  195.9 19.2 %copy-start.8 = (f32[1024]{0:T(1024)S(1)}, f32[1024]{0:T(1024)}, u32[]{:S(2)}) copy-start(f32[1024]{0:T(1024)} %param.25) | copy-start | bytes 12292
Sparse Core Ops, SparseCore 0:
  10.9 34.0 all-gather.4
  124.0 48.2 all-gather.6
